TPU v7x, 32 devices: a whole 2x2x4 slice. The times are simulated.
32 devices in a mesh: rep: 2 (over x), fs: 8 (over z, y), tp: 2 (over core).
Axes of the slice: x: 2, y: 2, z: 4, core: 2. Of those that a mesh axis runs over, the one named last changes fastest.
Arguments:
- inputs: bfloat16 [2, 3072, 2048], P('rep', 'fs', 'tp'), may hold values from -6 to 6
- gate_proj: bfloat16 [2048, 2816], P('fs', 'tp'), may hold values from -0.125 to 0.125
- value_proj: bfloat16 [2048, 2816], P('fs', 'tp'), may hold values from -0.125 to 0.125
- gate_taps: float32 [3, 2816], replicated, may hold values from -3 to 3
- value_taps: float32 [3, 2816], replicated, may hold values from -3 to 3
- out_grad: bfloat16 [2, 3072, 2816], P('rep', 'fs', 'tp'), may hold values from -6 to 6
Outputs:
- in_grad: bfloat16 [2, 3072, 2048], P('rep', 'fs', 'tp')
- gate_proj_grad: float32 [2048, 2816], P('fs', 'tp')
- value_proj_grad: float32 [2048, 2816], P('fs', 'tp')
- gate_taps_grad: float32 [3, 2816], replicated
- value_taps_grad: float32 [3, 2816], replicated
All inputs are finite; a program needn't handle non-finite values.
Results may differ from a plain program's by a relative error of at most 0.013.
Values may be sent and summed in bfloat16 or wider, within the bound.
A program may use at most 128 MiB of HBM per device.

v0:
```python
import jax
import jax.numpy as jnp
from jax import lax
from jax.sharding import PartitionSpec as P

HALO = 8


def shift(x, axis, step):
    count = lax.axis_size(axis)
    return lax.ppermute(x, axis, [(i, (i + step) % count) for i in range(count)])


def with_halo(rows):
    count = lax.axis_size("fs")
    nxt = lax.ppermute(rows[:HALO], "fs", [(i + 1, i) for i in range(count - 1)])
    prv = lax.ppermute(rows[rows.shape[0] - HALO :], "fs", [(i, i + 1) for i in range(count - 1)])
    return jnp.concatenate([rows, nxt, prv], axis=0)


def before(x):
    return jnp.concatenate([x[:, -1:], x[:, :-1]], axis=1)


def after(x):
    return jnp.concatenate([x[:, 1:], x[:, :1]], axis=1)


def shards(inputs, gate_proj, value_proj, gate_taps, value_taps, out_grad):
    contract_cols = (((1,), (1,)), ((), ()))
    contract_rows = (((0,), (0,)), ((), ()))
    reps, fs_count = (lax.axis_size("rep"), lax.axis_size("fs"))
    rep = lax.axis_index("rep")
    tokens, feats = inputs.shape[1:]
    hid = gate_proj.shape[1]
    width = min(hid, -(-hid // reps // 128) * 128)
    last = hid - width

    def start_of(part):
        return jnp.minimum(part * width, last)

    first = start_of(rep)
    dead = rep * width - first
    live = jnp.arange(width) >= dead

    def part_cols(x, part):
        return lax.dynamic_slice_in_dim(x, start_of(part), width, x.ndim - 1)

    w_own = jnp.concatenate(
        [
            jnp.where(live, part_cols(w, rep), jnp.zeros((), w.dtype))
            for w in (gate_proj, value_proj)
        ],
        axis=1,
    )
    w_all = lax.all_gather(w_own, "fs", axis=0, tiled=True)
    x_ext = with_halo(inputs[0])
    g_ext = with_halo(out_grad[0])
    x_blocks, g_blocks = ([x_ext], [part_cols(g_ext, rep)])
    for step in range(1, reps):
        x_blocks.append(shift(x_ext, "rep", step))
        g_blocks.append(shift(part_cols(g_ext, (rep + step) % reps), "rep", step))
    x_all = lax.all_gather(jnp.stack(x_blocks), "tp", axis=2, tiled=True)
    g_all = jnp.stack(g_blocks).astype(jnp.float32)
    ext = tokens + 2 * HALO
    pre = jnp.dot(x_all.reshape(reps * ext, -1), w_all, preferred_element_type=jnp.float32)
    pre = pre.astype(jnp.bfloat16).astype(jnp.float32).reshape(reps, ext, 2 * width)
    tap_start = lax.axis_index("tp") * hid + first
    taps = jnp.concatenate(
        [lax.dynamic_slice_in_dim(t, tap_start, width, 1) for t in (gate_taps, value_taps)], axis=1
    )
    pre_b, pre_a = (before(pre), after(pre))
    mix = taps[0] * pre_b + taps[1] * pre + taps[2] * pre_a
    gate_mix, value_mix = (mix[..., :width], mix[..., width:])
    sig = jax.nn.sigmoid(gate_mix)
    gate_cot = g_all * value_mix * (sig * (1.0 + gate_mix * (1.0 - sig)))
    value_cot = g_all * (gate_mix * sig)
    cot = jnp.concatenate([gate_cot, value_cot], axis=2)
    pre_cot = taps[0] * after(cot) + taps[1] * cot + taps[2] * before(cot)
    pre_cot = pre_cot[:, :tokens].astype(jnp.bfloat16).reshape(reps * tokens, 2 * width)
    tap_terms = jnp.stack(
        [jnp.sum(p[:, :tokens] * cot[:, :tokens], axis=(0, 1)) for p in (pre_b, pre, pre_a)]
    )
    factor = float(tokens * fs_count * reps) ** (-0.5)
    grads = lax.dot_general(
        x_all[:, :tokens].reshape(reps * tokens, -1),
        pre_cot,
        contract_rows,
        preferred_element_type=jnp.float32,
    )
    grads = (grads * factor).astype(jnp.bfloat16)
    own = lax.psum_scatter(grads, "fs", scatter_dimension=0, tiled=True)
    partial_value = lax.dot_general(
        pre_cot, w_all, contract_cols, preferred_element_type=jnp.float32
    )
    partial_value = lax.psum_scatter(
        partial_value.astype(jnp.bfloat16), "tp", scatter_dimension=1, tiled=True
    ).reshape(reps, tokens, feats)
    in_grad = partial_value[0].astype(jnp.float32)
    for step in range(1, reps):
        in_grad += shift(partial_value[step], "rep", -step).astype(jnp.float32)
    blocks = [own]
    for step in range(1, reps):
        blocks.append(shift(own, "rep", step))
    proj_grads = []
    for branch in range(2):
        cols = jnp.zeros((own.shape[0], hid), jnp.bfloat16)
        cut = [b[:, branch * width : (branch + 1) * width] for b in blocks]
        for step in range(reps):
            part = (rep - step) % reps
            place = start_of(part)
            skip = part * width - place
            old = lax.dynamic_slice_in_dim(cols, place, width, 1)
            new = jnp.where(jnp.arange(width) >= skip, cut[step], old)
            cols = lax.dynamic_update_slice_in_dim(cols, new, place, 1)
        proj_grads.append(cols.astype(jnp.float32))
    tap_sum = lax.psum(tap_terms * factor, "fs").reshape(3, 2, width)
    tap_all = lax.all_gather(lax.all_gather(tap_sum, "rep"), "tp")
    halves = []
    for half in range(tap_all.shape[0]):
        cols = [
            tap_all[half, p, :, :, max(0, p * width - last) if p * width > last else 0 :]
            for p in range(reps)
        ]
        halves.append(jnp.concatenate(cols, axis=2))
    taps_out = jnp.concatenate(halves, axis=2)
    return (
        in_grad.astype(jnp.bfloat16)[None],
        proj_grads[0],
        proj_grads[1],
        taps_out[:, 0],
        taps_out[:, 1],
    )


def solution(mesh):
    placed = (P("rep", "fs", "tp"), P("fs", "tp"), P("fs", "tp"), P(), P(), P("rep", "fs", "tp"))
    return jax.shard_map(
        shards,
        mesh=mesh,
        in_specs=placed,
        out_specs=(P("rep", "fs", "tp"), P("fs", "tp"), P("fs", "tp"), P(), P()),
        check_vma=False,
    )
```

profile of v0, /device:TPU:2, one launch (start us, length us, event | category | flops | bytes accessed | tf_op | source)
XLA Modules:
  0.0 368.1 jit_solution(3353467001362223861)
XLA Ops:
  7.2 0.0 all-gather.4.cloned.1.call-start
  7.2 1.5 copy.18
  8.7 0.1 slice_bitcast_fusion.1
  8.8 3.4 collective-permute-start.4
  12.3 1.3 collective-permute-start.3
  13.6 9.8 %collective-permute-done.4 = bf16[8,1024]{0,1:T(8,128)(2,1)S(1)} collective-permute-done((bf16[8,1024]{0,1:T(8,128)(2,1)S(1)}, bf16[8,1024]{0,1:T(8,128)(2,1)S(1)}, u32[]{:S(2)}, u32[]{:S(2)}) %collective-permute-start.4) | collective-permute-done | bytes 16416 | tf_op jit(solution)/shard_map/ppermute | solution.py:17
  23.4 0.2 pad_maximum_fusion.7
  23.6 0.5 copy.21
  24.1 0.6 collective-permute-start.5
  24.7 0.2 fusion.33
  24.9 16.7 %collective-permute-done.5 = bf16[400,1024]{1,0:T(8,128)(2,1)} collective-permute-done((bf16[400,1024]{1,0:T(8,128)(2,1)S(1)}, bf16[400,1024]{1,0:T(8,128)(2,1)}, u32[]{:S(2)}, u32[]{:S(2)}) %collective-permute-start.5) | collective-permute-done | bytes 819232 | tf_op jit(solution)/shard_map/ppermute | solution.py:11
  41.6 1.4 copy.22
  43.1 1.6 pad_maximum_fusion.4
  44.7 0.0 all-gather.4.cloned.1.call-update
  44.7 0.0 all-gather.6.cloned.1.call-start
  44.8 1.5 dynamic-slice_select_fusion.1
  46.3 0.9 pad_maximum_fusion.8
  47.2 0.0 all-gather.6.cloned.1.call-update
  47.2 0.0 reduce-scatter.3.cloned.1.call-start
  47.3 6.2 %collective-permute-start.1 = (bf16[8,1408]{1,0:T(8,128)(2,1)S(1)}, bf16[8,1408]{1,0:T(8,128)(2,1)S(1)}, u32[]{:S(2)}, u32[]{:S(2)}) collective-permute-start(bf16[8,1408]{1,0:T(8,128)(2,1)S(1)} %get-tuple-element.25), channel_id=1, source_target_pairs={{0,2},{2,4},{4,6},{6,8},{8,10},{10,12},{12,14},{1,3},{3,5},{5,7},{... | collective-permute-start | bytes 67592 | tf_op jit(solution)/shard_map/ppermute | solution.py:17
  53.5 1.5 collective-permute-start
  55.0 0.8 constant_dynamic-slice_fusion.1
  55.8 0.1 maximum_reduce_fusion.1
  55.9 4.8 %collective-permute-done = bf16[8,1408]{1,0:T(8,128)(2,1)S(1)} collective-permute-done((bf16[8,1408]{1,0:T(8,128)(2,1)S(1)}, bf16[8,1408]{1,0:T(8,128)(2,1)S(1)}, u32[]{:S(2)}, u32[]{:S(2)}) %collective-permute-start) | collective-permute-done | bytes 22560 | tf_op jit(solution)/shard_map/ppermute | solution.py:16
  60.6 0.1 pad_maximum_fusion.6
  60.7 1.6 dynamic-slice_bitcast_fusion
  62.3 0.6 collective-permute-start.2
  62.9 0.9 all-gather.4.cloned.1.call-done
  63.7 4.7 %copy.23 = bf16[2,400,2048]{2,1,0:T(8,128)(2,1)S(1)} copy(bf16[2,400,2048]{1,2,0:T(8,128)(2,1)} %all-gather.4.cloned.1.call-done) | data formatting | bytes 6553600 | tf_op jit(solution)/shard_map/all_gather | solution.py:63
  68.4 97.7 %all-gather.6.cloned.1.call-done = bf16[2048,1536]{1,0:T(8,128)(2,1)} async-done(((bf16[256,1536]{1,0:T(8,128)(2,1)}), bf16[2048,1536]{1,0:T(8,128)(2,1)}) %all-gather.6.cloned.1.call-update) | async-done | bytes 6291472 | tf_op jit(solution)/shard_map/all_gather | solution.py:56
  166.1 8.2 %convolution_convert_fusion = bf16[800,1536]{1,0:T(8,128)(2,1)S(1)} fusion(bf16[800,2048]{1,0:T(8,128)(2,1)S(1)} %bitcast.55, bf16[2048,1536]{1,0:T(8,128)(2,1)} %all-gather.6.cloned.1.call-done), kind=kOutput, calls=%fused_computation.37 | convolution fusion | flops 5034393600 | bytes 12025856 | tf_op jit(solution)/shard_map/dot_general | solution.py:66
  174.3 0.7 convert.5
  175.0 1.3 fusion.24
  176.3 0.0 copy-start
  176.3 1.7 fusion.3
  178.0 2.2 convert_multiply_fusion
  180.2 1.1 fusion.4
  181.3 8.2 %fusion.15 = (f32[1536]{0:T(1024)S(1)}, f32[1536]{0:T(1024)S(1)}, f32[1536]{0:T(1024)S(1)}, bf16[2,384,1536]{2,1,0:T(8,128)(2,1)S(1)}) fusion(f32[2,400,1536]{2,1,0:T(8,128)S(1)} %convert.5, f32[2,400,768]{2,1,0:T(8,128)S(1)} %get-tuple-element.11, f32[2,400,768]{2,1,0:T(8,128)S(1)} %get-tuple-element.12, f32[2,399,1536]{2,1,0:T(8,128)S(1)} %get-tuple-element.18, ...), kind=kLoop, calls=%fused_computation.31 | loop fusion | flops 20049408 | bytes 31494144 | tf_op jit(solution)/shard_map/reduce_sum | solution.py:82
  189.6 9.3 %convolution_convert_fusion.1 = bf16[768,2048]{1,0:T(8,128)(2,1)} fusion(bf16[768,1536]{1,0:T(8,128)(2,1)S(1)} %bitcast.56, bf16[2048,1536]{1,0:T(8,128)(2,1)} %all-gather.6.cloned.1.call-done), kind=kOutput, calls=%fused_computation.38 | convolution fusion | flops 4833411072 | bytes 11796480 | tf_op jit(solution)/shard_map/dot_general | solution.py:93
  198.9 0.0 reduce-scatter.3.cloned.1.call-update
  198.9 0.3 reduce-scatter.5.cloned.1.call-start
  199.2 8.9 %fusion = bf16[2048,1536]{1,0:T(8,128)(2,1)} fusion(bf16[2,384,1536]{2,1,0:T(8,128)(2,1)S(1)} %get-tuple-element.13, bf16[2,400,2048]{1,2,0:T(8,128)(2,1)} %all-gather.4.cloned.1.call-done), kind=kOutput, calls=%fused_computation.1 | convolution fusion | flops 4838129664 | bytes 11796480 | tf_op jit(solution)/shard_map/dot_general | solution.py:85
  208.1 0.0 reduce-scatter.5.cloned.1.call-update
  208.3 35.4 %psum.7 = f32[1,3,2,768]{3,2,1,0:T(2,128)S(1)} all-reduce(f32[1,3,2,768]{3,2,1,0:T(2,128)S(1)} %all_gather_reshape.3), channel_id=1, replica_groups=mesh['rep'=2,'fs'=8,'tp'=2] {'fs'}, use_global_device_ids=true, to_apply=%region_5.6 | all-reduce | flops 4608 | bytes 36864 | tf_op jit(solution)/shard_map/psum | solution.py:117
  243.7 4.4 %all_gather.17 = f32[2,3,2,768]{3,2,1,0:T(2,128)S(1)} all-gather(f32[1,3,2,768]{3,2,1,0:T(2,128)S(1)} %psum.7), channel_id=1, replica_groups=mesh['rep'=2,'fs'=8,'tp'=2] {'rep'}, dimensions={0}, use_global_device_ids=true | all-gather | bytes 55296 | tf_op jit(solution)/shard_map/all_gather | solution.py:118
  248.1 1.8 all-gather
  250.0 0.0 reduce-scatter.3.cloned.1.call-done
  250.0 1.2 slice.184
  251.3 0.8 collective-permute-start.6
  252.1 79.1 %reduce-scatter.5.cloned.1.call-done = bf16[256,1536]{1,0:T(8,128)(2,1)} async-done(((bf16[2048,1536]{1,0:T(8,128)(2,1)}), bf16[256,1536]{1,0:T(8,128)(2,1)}) %reduce-scatter.5.cloned.1.call-update) | async-done | bytes 786448 | tf_op jit(solution)/shard_map/reduce_scatter | solution.py:92
  331.2 0.6 collective-permute-start.7
  331.8 0.6 slice_bitcast_fusion.2
  332.4 2.3 fusion.20
  334.8 1.2 slice_select_fusion.1
  335.9 0.1 broadcast.11.clone
  336.0 3.1 dynamic_update_slice.12
  339.1 0.1 broadcast.11.clone.1
  339.2 3.1 dynamic_update_slice.14
  342.3 7.6 %collective-permute-done.7 = bf16[256,1536]{1,0:T(8,128)(2,1)S(1)} collective-permute-done((bf16[256,1536]{1,0:T(8,128)(2,1)}, bf16[256,1536]{1,0:T(8,128)(2,1)S(1)}, u32[]{:S(2)}, u32[]{:S(2)}) %collective-permute-start.7) | collective-permute-done | bytes 786464 | tf_op jit(solution)/shard_map/ppermute | solution.py:11
  349.9 0.4 slice_select_fusion
  350.4 4.4 %dynamic_update_slice.13 = bf16[256,1408]{1,0:T(8,128)(2,1)S(1)} dynamic-update-slice(bf16[256,1408]{1,0:T(8,128)(2,1)S(1)} %dynamic_update_slice.12, bf16[256,768]{1,0:T(8,128)(2,1)S(1)} %get-tuple-element.27, s32[]{:T(128)} %constant.42.clone.1, s32[]{:T(128)S(6)} %select_n.71) | dynamic-update-slice | bytes 786436 | tf_op jit(solution)/shard_map/dynamic_update_slice | solution.py:115
  354.8 1.2 convert_element_type.36
  356.0 4.3 %dynamic_update_slice.15 = bf16[256,1408]{1,0:T(8,128)(2,1)S(1)} dynamic-update-slice(bf16[256,1408]{1,0:T(8,128)(2,1)S(1)} %dynamic_update_slice.14, bf16[256,768]{1,0:T(8,128)(2,1)S(1)} %get-tuple-element.26, s32[]{:T(128)} %constant.42.clone.1, s32[]{:T(128)S(6)} %select_n.71) | dynamic-update-slice | bytes 786436 | tf_op jit(solution)/shard_map/dynamic_update_slice | solution.py:115
  360.4 1.2 convert_element_type.37
  (25 shorter events, 0.2 us)
Async XLA Ops:
  7.2 56.6 %all-gather.4.cloned.1.call-start = ((), (), s32[]{:S(2)}) async-start(), calls=%async_computation.2 | async-start | bytes 6291456 | tf_op jit(solution)/shard_map/all_gather | solution.py:63
  8.8 14.6 %collective-permute-start.4 = (bf16[8,1024]{0,1:T(8,128)(2,1)S(1)}, bf16[8,1024]{0,1:T(8,128)(2,1)S(1)}, u32[]{:S(2)}, u32[]{:S(2)}) collective-permute-start(bf16[8,1024]{0,1:T(8,128)(2,1)S(1)} %get-tuple-element.31), channel_id=1, source_target_pairs={{0,2},{2,4},{4,6},{6,8},{8,10},{10,12},{12,14},{1,3},{3,5},{5,7},{... | collective-permute-start | bytes 49160 | tf_op jit(solution)/shard_map/ppermute | solution.py:17
  12.3 11.2 %collective-permute-start.3 = (bf16[8,1024]{0,1:T(8,128)(2,1)S(1)}, bf16[8,1024]{0,1:T(8,128)(2,1)S(1)}, u32[]{:S(2)}, u32[]{:S(2)}) collective-permute-start(bf16[8,1024]{0,1:T(8,128)(2,1)S(1)} %get-tuple-element.30), channel_id=1, source_target_pairs={{2,0},{4,2},{6,4},{8,6},{10,8},{12,10},{14,12},{3,1},{5,3},{7,5},{... | collective-permute-start | bytes 49160 | tf_op jit(solution)/shard_map/ppermute | solution.py:16
  24.1 17.5 %collective-permute-start.5 = (bf16[400,1024]{1,0:T(8,128)(2,1)S(1)}, bf16[400,1024]{1,0:T(8,128)(2,1)}, u32[]{:S(2)}, u32[]{:S(2)}) collective-permute-start(bf16[400,1024]{1,0:T(8,128)(2,1)S(1)} %copy.21), channel_id=1, source_target_pairs={{0,16},{16,0},{1,17},{17,1},{2,18},{18,2},{3,19},{19,3},{4,20},{20... | collective-permute-start | bytes 2457608 | tf_op jit(solution)/shard_map/ppermute | solution.py:11
  43.1 4.2 %copy-start.1 = (bf16[1,384,1408]{2,1,0:T(8,128)(2,1)S(1)}, bf16[1,384,1408]{2,1,0:T(8,128)(2,1)}, u32[]{:S(2)}) copy-start(bf16[1,384,1408]{2,1,0:T(8,128)(2,1)} %param.11) | copy-start | bytes 3244036
  44.7 121.4 %all-gather.6.cloned.1.call-start = ((), (), s32[]{:S(2)}) async-start(), calls=%async_computation.3 | async-start | bytes 7077888 | tf_op jit(solution)/shard_map/all_gather | solution.py:56
  47.2 202.8 %reduce-scatter.3.cloned.1.call-start = ((), (), s32[]{:S(2)}) async-start(), calls=%async_computation.4 | async-start | bytes 4718592 | tf_op jit(solution)/shard_map/reduce_scatter | solution.py:96
  47.3 8.5 %collective-permute-start.1 = (bf16[8,1408]{1,0:T(8,128)(2,1)S(1)}, bf16[8,1408]{1,0:T(8,128)(2,1)S(1)}, u32[]{:S(2)}, u32[]{:S(2)}) collective-permute-start(bf16[8,1408]{1,0:T(8,128)(2,1)S(1)} %get-tuple-element.25), channel_id=1, source_target_pairs={{0,2},{2,4},{4,6},{6,8},{8,10},{10,12},{12,14},{1,3},{3,5},{5,7},{... | collective-permute-start | bytes 67592 | tf_op jit(solution)/shard_map/ppermute | solution.py:17
  53.5 7.1 %collective-permute-start = (bf16[8,1408]{1,0:T(8,128)(2,1)S(1)}, bf16[8,1408]{1,0:T(8,128)(2,1)S(1)}, u32[]{:S(2)}, u32[]{:S(2)}) collective-permute-start(bf16[8,1408]{1,0:T(8,128)(2,1)S(1)} %get-tuple-element.24), channel_id=1, source_target_pairs={{2,0},{4,2},{6,4},{8,6},{10,8},{12,10},{14,12},{3,1},{5,3},{7,5},{... | collective-permute-start | bytes 67592 | tf_op jit(solution)/shard_map/ppermute | solution.py:16
  62.3 115.7 %collective-permute-start.2 = (bf16[400,768]{1,0:T(8,128)(2,1)}, bf16[400,768]{1,0:T(8,128)(2,1)}, u32[]{:S(2)}, u32[]{:S(2)}) collective-permute-start(bf16[400,768]{1,0:T(8,128)(2,1)} %get-tuple-element.23), channel_id=1, source_target_pairs={{0,16},{16,0},{1,17},{17,1},{2,18},{18,2},{3,19},{19,3},{4,20},{20... | collective-permute-start | bytes 1843208 | tf_op jit(solution)/shard_map/ppermute | solution.py:11
  176.3 1.7 copy-start
  198.9 132.3 %reduce-scatter.5.cloned.1.call-start = ((), (), s32[]{:S(2)}) async-start(), calls=%async_computation.5 | async-start | bytes 7077888 | tf_op jit(solution)/shard_map/reduce_scatter | solution.py:92
  251.3 81.2 %collective-permute-start.6 = (bf16[384,1024]{1,0:T(8,128)(2,1)S(1)}, bf16[384,1024]{1,0:T(8,128)(2,1)S(1)}, u32[]{:S(2)}, u32[]{:S(2)}) collective-permute-start(bf16[384,1024]{1,0:T(8,128)(2,1)S(1)} %slice.184), channel_id=1, source_target_pairs={{0,16},{16,0},{1,17},{17,1},{2,18},{18,2},{3,19},{19,3},{4,20},{20... | collective-permute-start | bytes 2359304 | tf_op jit(solution)/shard_map/ppermute | solution.py:11
  331.2 18.7 %collective-permute-start.7 = (bf16[256,1536]{1,0:T(8,128)(2,1)}, bf16[256,1536]{1,0:T(8,128)(2,1)S(1)}, u32[]{:S(2)}, u32[]{:S(2)}) collective-permute-start(bf16[256,1536]{1,0:T(8,128)(2,1)} %reduce-scatter.5.cloned.1.call-done), channel_id=1, source_target_pairs={{0,16},{16,0},{1,17},{17,1},{2,18},{18,2},{3,19},{19,3},{4,20},{20... | collective-permute-start | bytes 2359304 | tf_op jit(solution)/shard_map/ppermute | solution.py:11
Sparse Core Ops, SparseCore 0:
  44.8 18.8 all-gather.3
  66.5 99.5 all-gather.5
  199.0 9.4 reduce-scatter.2
  212.0 119.1 reduce-scatter.4
where the time goes:
time: 369 us; the launch traced here: 368 us
  waiting for transfers between devices  217 us (59%)
  blocking collectives  41.6 us (11%)
  local copies, waits for them, and re-layouts  29 us (8%)
  matrix products  26.4 us (7%)
  other arithmetic  24.7 us (7%)
  starting transfers between devices  15.3 us (4%)
  between operations  14.2 us (4%)
    all_gather x1, waiting for transfers between devices, shards(): w_all = lax.all_gather(w_own, 'fs', axis=0, tiled=True)  97.7 us
    reduce_scatter x1, waiting for transfers between devices, shards(): own = lax.psum_scatter(grads, 'fs', scatter_dimension=0, tiled=True)  79.1 us
    psum x1, blocking collectives, shards(): tap_sum = lax.psum(tap_terms * factor, 'fs').reshape(3, 2, width)  35.4 us
    ppermute x4, waiting for transfers between devices, shift(): lax.ppermute(x, axis, [(i, (i + step) % count) for i in range(count)])  24.4 us
    dynamic_update_slice x4, local copies, waits for them, and re-layouts, shards(): cols = lax.dynamic_update_slice_in_dim(cols, new, place, 1)  15 us
    ppermute x2, waiting for transfers between devices, with_halo(): lax.ppermute(rows[rows.shape[0] - HALO:], 'fs', [(i, i + 1) for i in rang...  9.85 us
    ppermute x2, starting transfers between devices, with_halo(): lax.ppermute(rows[rows.shape[0] - HALO:], 'fs', [(i, i + 1) for i in rang...  9.6 us
    dot_general x1, matrix products, shards(): lax.dot_general(pre_cot, w_all, contract_cols, preferred_element_type=jnp...  9.31 us
  transfers between devices with their start and end apart: 12, of which 7 were waited for; matrix products, arithmetic and copies ran while one was open for 12% of the time, Pallas kernels for 0%

commit v1 on v0

--- a/solution.py
+++ b/solution.py
@@ -53,7 +53,10 @@
         ],
         axis=1,
     )
-    w_all = lax.all_gather(w_own, "fs", axis=0, tiled=True)
+    n_dev = lax.axis_size("fs")
+    pieces = jnp.stack([w_own for _ in range(n_dev)])
+    pieces = lax.all_to_all(pieces, "fs", split_axis=0, concat_axis=0)
+    w_all = jnp.concatenate(pieces, axis=0)
     x_ext = with_halo(inputs[0])
     g_ext = with_halo(out_grad[0])
     x_blocks, g_blocks = ([x_ext], [part_cols(g_ext, rep)])

time: 369 us -> 409 us (1.11)
  starting transfers between devices: 15.3 us -> 69.6 us
  waiting for transfers between devices: 217 us -> 197 us
    all_gather x1 -> x0, waiting for transfers between devices: 97.7 us -> none  [shards(): w_all = lax.all_gather(w_own, 'fs', axis=0, tiled=True)]
    ppermute x2, starting transfers between devices: 9.6 us -> 58 us  [with_halo(): lax.ppermute(rows[rows.shape[0] - HALO:], 'fs', [(i, i + 1) for i in rang...]
    ppermute x2, waiting for transfers between devices: 9.85 us -> 52.8 us  [with_halo(): lax.ppermute(rows[rows.shape[0] - HALO:], 'fs', [(i, i + 1) for i in rang...]
    all_gather x1, waiting for transfers between devices: 0.86 us -> 34.2 us  [shards(): x_all = lax.all_gather(jnp.stack(x_blocks), 'tp', axis=2, tiled=True)]
    all_to_all x0 -> x1, starting transfers between devices: none -> 5.97 us  [shards(): pieces = lax.all_to_all(pieces, 'fs', split_axis=0, concat_axis=0)]
  transfers between devices with their start and end apart: 12 -> 12, of which waited for: 7 -> 6; matrix products, arithmetic and copies ran while one was open for 12% -> 11% of each run, Pallas kernels for 0% -> 0%
where the time goes in v1:
time: 409 us; the launch traced here: 408 us
  waiting for transfers between devices  197 us (48%)
  starting transfers between devices  69.6 us (17%)
  blocking collectives  44.4 us (11%)
  local copies, waits for them, and re-layouts  31.8 us (8%)
  matrix products  26.5 us (6%)
  other arithmetic  24.8 us (6%)
  between operations  14.2 us (3%)
    reduce_scatter x1, waiting for transfers between devices, shards(): own = lax.psum_scatter(grads, 'fs', scatter_dimension=0, tiled=True)  79.3 us
    ppermute x2, starting transfers between devices, with_halo(): lax.ppermute(rows[rows.shape[0] - HALO:], 'fs', [(i, i + 1) for i in rang...  58 us
    ppermute x2, waiting for transfers between devices, with_halo(): lax.ppermute(rows[rows.shape[0] - HALO:], 'fs', [(i, i + 1) for i in rang...  52.8 us
    psum x1, blocking collectives, shards(): tap_sum = lax.psum(tap_terms * factor, 'fs').reshape(3, 2, width)  38.2 us
    all_gather x1, waiting for transfers between devices, shards(): x_all = lax.all_gather(jnp.stack(x_blocks), 'tp', axis=2, tiled=True)  34.2 us
    ppermute x4, waiting for transfers between devices, shift(): lax.ppermute(x, axis, [(i, (i + step) % count) for i in range(count)])  25.4 us
    dynamic_update_slice x4, local copies, waits for them, and re-layouts, shards(): cols = lax.dynamic_update_slice_in_dim(cols, new, place, 1)  15 us
    dot_general x1, matrix products, shards(): lax.dot_general(pre_cot, w_all, contract_cols, preferred_element_type=jnp...  9.33 us
  transfers between devices with their start and end apart: 12, of which 6 were waited for; matrix products, arithmetic and copies ran while one was open for 11% of the time, Pallas kernels for 0%

profile of v1, /device:TPU:2, one launch (start us, length us, event | category | flops | bytes accessed | tf_op | source)
XLA Modules:
  0.0 408.5 jit_solution(7205016108748961164)
XLA Ops:
  7.2 1.5 dynamic-slice_select_fusion.1
  8.7 0.1 pad_maximum_fusion.8
  8.8 3.2 stack.47
  11.9 6.0 %all-to-all-start = ((bf16[8,256,1536]{2,1,0:T(8,128)(2,1)}), bf16[8,256,1536]{2,1,0:T(8,128)(2,1)}, u32[]{:S(2)}, u32[]{:S(2)}) async-start(bf16[8,256,1536]{2,1,0:T(8,128)(2,1)} %stack.47), calls=%async_computation | async-start | bytes 12582912 | tf_op jit(solution)/shard_map/all_to_all | solution.py:58
  17.9 0.0 all-gather.3.cloned.1.call-start
  17.9 0.4 copy.18
  18.3 0.1 slice_bitcast_fusion.1
  18.4 3.9 collective-permute-start.4
  22.4 1.3 collective-permute-start.3
  23.7 52.8 %collective-permute-done.4 = bf16[8,1024]{0,1:T(8,128)(2,1)S(1)} collective-permute-done((bf16[8,1024]{0,1:T(8,128)(2,1)S(1)}, bf16[8,1024]{0,1:T(8,128)(2,1)S(1)}, u32[]{:S(2)}, u32[]{:S(2)}) %collective-permute-start.4) | collective-permute-done | bytes 16416 | tf_op jit(solution)/shard_map/ppermute | solution.py:17
  76.5 0.0 collective-permute-done.3
  76.5 0.2 pad_maximum_fusion.7
  76.7 1.2 copy.21
  77.9 0.6 collective-permute-start.5
  78.5 1.1 fusion.33
  79.6 17.7 %collective-permute-done.5 = bf16[400,1024]{1,0:T(8,128)(2,1)} collective-permute-done((bf16[400,1024]{1,0:T(8,128)(2,1)}, bf16[400,1024]{1,0:T(8,128)(2,1)}, u32[]{:S(2)}, u32[]{:S(2)}) %collective-permute-start.5) | collective-permute-done | bytes 819232 | tf_op jit(solution)/shard_map/ppermute | solution.py:11
  97.4 1.4 copy.22
  98.8 1.6 pad_maximum_fusion.4
  100.4 0.0 all-gather.3.cloned.1.call-update
  100.4 0.0 reduce-scatter.3.cloned.1.call-start
  100.5 54.1 %collective-permute-start.1 = (bf16[8,1408]{1,0:T(8,128)(2,1)S(1)}, bf16[8,1408]{1,0:T(8,128)(2,1)S(1)}, u32[]{:S(2)}, u32[]{:S(2)}) collective-permute-start(bf16[8,1408]{1,0:T(8,128)(2,1)S(1)} %get-tuple-element.25), channel_id=1, source_target_pairs={{0,2},{2,4},{4,6},{6,8},{8,10},{10,12},{12,14},{1,3},{3,5},{5,7},{... | collective-permute-start | bytes 67592 | tf_op jit(solution)/shard_map/ppermute | solution.py:17
  154.6 1.5 collective-permute-start
  156.1 0.8 constant_dynamic-slice_fusion.1
  156.9 0.1 maximum_reduce_fusion.1
  156.9 5.4 %collective-permute-done = bf16[8,1408]{1,0:T(8,128)(2,1)S(1)} collective-permute-done((bf16[8,1408]{1,0:T(8,128)(2,1)S(1)}, bf16[8,1408]{1,0:T(8,128)(2,1)S(1)}, u32[]{:S(2)}, u32[]{:S(2)}) %collective-permute-start) | collective-permute-done | bytes 22560 | tf_op jit(solution)/shard_map/ppermute | solution.py:16
  162.4 0.1 pad_maximum_fusion.6
  162.4 1.6 dynamic-slice_bitcast_fusion
  164.0 0.6 collective-permute-start.2
  164.6 34.2 %all-gather.3.cloned.1.call-done = bf16[2,400,2048]{1,2,0:T(8,128)(2,1)} async-done(((bf16[2,400,1024]{1,2,0:T(8,128)(2,1)}), bf16[2,400,2048]{1,2,0:T(8,128)(2,1)}) %all-gather.3.cloned.1.call-update) | async-done | bytes 3276816 | tf_op jit(solution)/shard_map/all_gather | solution.py:66
  198.8 4.7 %copy.23 = bf16[2,400,2048]{2,1,0:T(8,128)(2,1)S(1)} copy(bf16[2,400,2048]{1,2,0:T(8,128)(2,1)} %all-gather.3.cloned.1.call-done) | data formatting | bytes 6553600 | tf_op jit(solution)/shard_map/all_gather | solution.py:66
  203.5 8.2 %convolution_convert_fusion = bf16[800,1536]{1,0:T(8,128)(2,1)S(1)} fusion(bf16[800,2048]{1,0:T(8,128)(2,1)S(1)} %bitcast.56, bf16[2048,1536]{1,0:T(8,128)(2,1)} %bitcast.11), kind=kOutput, calls=%fused_computation.37 | convolution fusion | flops 5034393600 | bytes 12025856 | tf_op jit(solution)/shard_map/dot_general | solution.py:69
  211.7 0.7 convert.5
  212.4 1.3 fusion.24
  213.7 0.0 copy-start
  213.7 1.7 fusion.3
  215.4 2.2 convert_multiply_fusion
  217.7 1.1 fusion.4
  218.8 8.2 %fusion.15 = (f32[1536]{0:T(1024)S(1)}, f32[1536]{0:T(1024)S(1)}, f32[1536]{0:T(1024)S(1)}, bf16[2,384,1536]{2,1,0:T(8,128)(2,1)S(1)}) fusion(f32[2,400,1536]{2,1,0:T(8,128)S(1)} %convert.5, f32[2,400,768]{2,1,0:T(8,128)S(1)} %get-tuple-element.11, f32[2,400,768]{2,1,0:T(8,128)S(1)} %get-tuple-element.12, f32[2,399,1536]{2,1,0:T(8,128)S(1)} %get-tuple-element.18, ...), kind=kLoop, calls=%fused_computation.31 | loop fusion | flops 20049408 | bytes 31494144 | tf_op jit(solution)/shard_map/reduce_sum | solution.py:85
  227.0 9.3 %convolution_convert_fusion.1 = bf16[768,2048]{1,0:T(8,128)(2,1)} fusion(bf16[768,1536]{1,0:T(8,128)(2,1)S(1)} %bitcast.57, bf16[2048,1536]{1,0:T(8,128)(2,1)} %bitcast.11), kind=kOutput, calls=%fused_computation.38 | convolution fusion | flops 4833411072 | bytes 11796480 | tf_op jit(solution)/shard_map/dot_general | solution.py:96
  236.3 0.0 reduce-scatter.3.cloned.1.call-update
  236.3 0.3 reduce-scatter.5.cloned.1.call-start
  236.6 9.0 %fusion = bf16[2048,1536]{1,0:T(8,128)(2,1)} fusion(bf16[2,384,1536]{2,1,0:T(8,128)(2,1)S(1)} %get-tuple-element.13, bf16[2,400,2048]{1,2,0:T(8,128)(2,1)} %all-gather.3.cloned.1.call-done), kind=kOutput, calls=%fused_computation.1 | convolution fusion | flops 4838129664 | bytes 11796480 | tf_op jit(solution)/shard_map/dot_general | solution.py:88
  245.6 0.0 reduce-scatter.5.cloned.1.call-update
  245.8 38.2 %psum.7 = f32[1,3,2,768]{3,2,1,0:T(2,128)S(1)} all-reduce(f32[1,3,2,768]{3,2,1,0:T(2,128)S(1)} %all_gather_reshape.3), channel_id=1, replica_groups=mesh['rep'=2,'fs'=8,'tp'=2] {'fs'}, use_global_device_ids=true, to_apply=%region_5.6 | all-reduce | flops 4608 | bytes 36864 | tf_op jit(solution)/shard_map/psum | solution.py:120
  283.9 4.4 %all_gather.13 = f32[2,3,2,768]{3,2,1,0:T(2,128)S(1)} all-gather(f32[1,3,2,768]{3,2,1,0:T(2,128)S(1)} %psum.7), channel_id=1, replica_groups=mesh['rep'=2,'fs'=8,'tp'=2] {'rep'}, dimensions={0}, use_global_device_ids=true | all-gather | bytes 55296 | tf_op jit(solution)/shard_map/all_gather | solution.py:121
  288.4 1.8 all-gather
  290.3 0.0 reduce-scatter.3.cloned.1.call-done
  290.3 1.2 slice.184
  291.5 0.8 collective-permute-start.6
  292.4 79.3 %reduce-scatter.5.cloned.1.call-done = bf16[256,1536]{1,0:T(8,128)(2,1)} async-done(((bf16[2048,1536]{1,0:T(8,128)(2,1)}), bf16[256,1536]{1,0:T(8,128)(2,1)}) %reduce-scatter.5.cloned.1.call-update) | async-done | bytes 786448 | tf_op jit(solution)/shard_map/reduce_scatter | solution.py:95
  371.6 0.6 collective-permute-start.7
  372.2 0.6 slice_bitcast_fusion.2
  372.9 2.3 fusion.20
  375.2 1.2 slice_select_fusion.1
  376.3 0.1 broadcast.13.clone
  376.4 3.1 dynamic_update_slice.12
  379.5 0.1 broadcast.13.clone.1
  379.6 3.1 dynamic_update_slice.14
  382.7 7.6 %collective-permute-done.7 = bf16[256,1536]{1,0:T(8,128)(2,1)S(1)} collective-permute-done((bf16[256,1536]{1,0:T(8,128)(2,1)}, bf16[256,1536]{1,0:T(8,128)(2,1)S(1)}, u32[]{:S(2)}, u32[]{:S(2)}) %collective-permute-start.7) | collective-permute-done | bytes 786464 | tf_op jit(solution)/shard_map/ppermute | solution.py:11
  390.3 0.4 slice_select_fusion
  390.8 4.4 %dynamic_update_slice.13 = bf16[256,1408]{1,0:T(8,128)(2,1)S(1)} dynamic-update-slice(bf16[256,1408]{1,0:T(8,128)(2,1)S(1)} %dynamic_update_slice.12, bf16[256,768]{1,0:T(8,128)(2,1)S(1)} %get-tuple-element.27, s32[]{:T(128)} %constant.42.clone.1, s32[]{:T(128)S(6)} %select_n.71) | dynamic-update-slice | bytes 786436 | tf_op jit(solution)/shard_map/dynamic_update_slice | solution.py:118
  395.2 1.2 convert_element_type.36
  396.4 4.3 %dynamic_update_slice.15 = bf16[256,1408]{1,0:T(8,128)(2,1)S(1)} dynamic-update-slice(bf16[256,1408]{1,0:T(8,128)(2,1)S(1)} %dynamic_update_slice.14, bf16[256,768]{1,0:T(8,128)(2,1)S(1)} %get-tuple-element.26, s32[]{:T(128)} %constant.42.clone.1, s32[]{:T(128)S(6)} %select_n.71) | dynamic-update-slice | bytes 786436 | tf_op jit(solution)/shard_map/dynamic_update_slice | solution.py:118
  400.8 1.2 convert_element_type.37
  (29 shorter events, 0.2 us)
Async XLA Ops:
  11.9 6.0 %copy-start.3 = (bf16[1,384,1024]{2,1,0:T(8,128)(2,1)S(1)}, bf16[1,384,1024]{2,1,0:T(8,128)(2,1)}, u32[]{:S(2)}) copy-start(bf16[1,384,1024]{2,1,0:T(8,128)(2,1)} %param.6) | copy-start | bytes 2359300
  11.9 191.6 %all-to-all-start = ((bf16[8,256,1536]{2,1,0:T(8,128)(2,1)}), bf16[8,256,1536]{2,1,0:T(8,128)(2,1)}, u32[]{:S(2)}, u32[]{:S(2)}) async-start(bf16[8,256,1536]{2,1,0:T(8,128)(2,1)} %stack.47), calls=%async_computation | async-start | bytes 12582912 | tf_op jit(solution)/shard_map/all_to_all | solution.py:58
  17.9 180.9 %all-gather.3.cloned.1.call-start = ((), (), s32[]{:S(2)}) async-start(), calls=%async_computation.3 | async-start | bytes 6291456 | tf_op jit(solution)/shard_map/all_gather | solution.py:66
  18.4 58.0 %collective-permute-start.4 = (bf16[8,1024]{0,1:T(8,128)(2,1)S(1)}, bf16[8,1024]{0,1:T(8,128)(2,1)S(1)}, u32[]{:S(2)}, u32[]{:S(2)}) collective-permute-start(bf16[8,1024]{0,1:T(8,128)(2,1)S(1)} %get-tuple-element.31), channel_id=1, source_target_pairs={{0,2},{2,4},{4,6},{6,8},{8,10},{10,12},{12,14},{1,3},{3,5},{5,7},{... | collective-permute-start | bytes 49160 | tf_op jit(solution)/shard_map/ppermute | solution.py:17
  22.4 54.1 %collective-permute-start.3 = (bf16[8,1024]{0,1:T(8,128)(2,1)S(1)}, bf16[8,1024]{0,1:T(8,128)(2,1)S(1)}, u32[]{:S(2)}, u32[]{:S(2)}) collective-permute-start(bf16[8,1024]{0,1:T(8,128)(2,1)S(1)} %get-tuple-element.30), channel_id=1, source_target_pairs={{2,0},{4,2},{6,4},{8,6},{10,8},{12,10},{14,12},{3,1},{5,3},{7,5},{... | collective-permute-start | bytes 49160 | tf_op jit(solution)/shard_map/ppermute | solution.py:16
  76.5 1.4 copy-start.2
  77.9 22.5 %copy-start.1 = (bf16[1,384,1408]{2,1,0:T(8,128)(2,1)S(1)}, bf16[1,384,1408]{2,1,0:T(8,128)(2,1)}, u32[]{:S(2)}) copy-start(bf16[1,384,1408]{2,1,0:T(8,128)(2,1)} %param.11) | copy-start | bytes 3244036
  77.9 19.4 %collective-permute-start.5 = (bf16[400,1024]{1,0:T(8,128)(2,1)}, bf16[400,1024]{1,0:T(8,128)(2,1)}, u32[]{:S(2)}, u32[]{:S(2)}) collective-permute-start(bf16[400,1024]{1,0:T(8,128)(2,1)} %copy.21), channel_id=1, source_target_pairs={{0,16},{16,0},{1,17},{17,1},{2,18},{18,2},{3,19},{19,3},{4,20},{20... | collective-permute-start | bytes 2457608 | tf_op jit(solution)/shard_map/ppermute | solution.py:11
  100.4 189.9 %reduce-scatter.3.cloned.1.call-start = ((), (), s32[]{:S(2)}) async-start(), calls=%async_computation.4 | async-start | bytes 4718592 | tf_op jit(solution)/shard_map/reduce_scatter | solution.py:99
  100.5 56.5 %collective-permute-start.1 = (bf16[8,1408]{1,0:T(8,128)(2,1)S(1)}, bf16[8,1408]{1,0:T(8,128)(2,1)S(1)}, u32[]{:S(2)}, u32[]{:S(2)}) collective-permute-start(bf16[8,1408]{1,0:T(8,128)(2,1)S(1)} %get-tuple-element.25), channel_id=1, source_target_pairs={{0,2},{2,4},{4,6},{6,8},{8,10},{10,12},{12,14},{1,3},{3,5},{5,7},{... | collective-permute-start | bytes 67592 | tf_op jit(solution)/shard_map/ppermute | solution.py:17
  154.6 7.8 %collective-permute-start = (bf16[8,1408]{1,0:T(8,128)(2,1)S(1)}, bf16[8,1408]{1,0:T(8,128)(2,1)S(1)}, u32[]{:S(2)}, u32[]{:S(2)}) collective-permute-start(bf16[8,1408]{1,0:T(8,128)(2,1)S(1)} %get-tuple-element.24), channel_id=1, source_target_pairs={{2,0},{4,2},{6,4},{8,6},{10,8},{12,10},{14,12},{3,1},{5,3},{7,5},{... | collective-permute-start | bytes 67592 | tf_op jit(solution)/shard_map/ppermute | solution.py:16
  164.0 51.4 %collective-permute-start.2 = (bf16[400,768]{1,0:T(8,128)(2,1)}, bf16[400,768]{1,0:T(8,128)(2,1)}, u32[]{:S(2)}, u32[]{:S(2)}) collective-permute-start(bf16[400,768]{1,0:T(8,128)(2,1)} %get-tuple-element.23), channel_id=1, source_target_pairs={{0,16},{16,0},{1,17},{17,1},{2,18},{18,2},{3,19},{19,3},{4,20},{20... | collective-permute-start | bytes 1843208 | tf_op jit(solution)/shard_map/ppermute | solution.py:11
  213.7 1.7 copy-start
  236.3 135.3 %reduce-scatter.5.cloned.1.call-start = ((), (), s32[]{:S(2)}) async-start(), calls=%async_computation.5 | async-start | bytes 7077888 | tf_op jit(solution)/shard_map/reduce_scatter | solution.py:95
  291.5 81.3 %collective-permute-start.6 = (bf16[384,1024]{1,0:T(8,128)(2,1)S(1)}, bf16[384,1024]{1,0:T(8,128)(2,1)S(1)}, u32[]{:S(2)}, u32[]{:S(2)}) collective-permute-start(bf16[384,1024]{1,0:T(8,128)(2,1)S(1)} %slice.184), channel_id=1, source_target_pairs={{0,16},{16,0},{1,17},{17,1},{2,18},{18,2},{3,19},{19,3},{4,20},{20... | collective-permute-start | bytes 2359304 | tf_op jit(solution)/shard_map/ppermute | solution.py:11
  371.6 18.7 %collective-permute-start.7 = (bf16[256,1536]{1,0:T(8,128)(2,1)}, bf16[256,1536]{1,0:T(8,128)(2,1)S(1)}, u32[]{:S(2)}, u32[]{:S(2)}) collective-permute-start(bf16[256,1536]{1,0:T(8,128)(2,1)} %reduce-scatter.5.cloned.1.call-done), channel_id=1, source_target_pairs={{0,16},{16,0},{1,17},{17,1},{2,18},{18,2},{3,19},{19,3},{4,20},{20... | collective-permute-start | bytes 2359304 | tf_op jit(solution)/shard_map/ppermute | solution.py:11
Sparse Core Ops, SparseCore 0:
  100.5 98.2 all-gather.2
  236.5 12.2 reduce-scatter.2
  252.3 119.2 reduce-scatter.4
